TPU v7x, 32 devices: a whole 2x2x4 slice. The times are simulated.
32 devices in a mesh: ep: 8 (over z, y), tp: 4 (over x, core).
Axes of the slice: x: 2, y: 2, z: 4, core: 2. Of those that a mesh axis runs over, the one named last changes fastest.
Arguments:
- mixer_input: bfloat16 [4096, 2048], P('ep'), may hold values from -6 to 6
- log_forget_total: float32 [16, 4096], P('tp'), may hold values from -684 to 0, as said below
- mixer_gain: float32 [2048], replicated, may hold values from 0.1 to 1.9
- w_query: bfloat16 [2048, 1024], P(None, 'tp'), may hold values from -1 to 1
- w_key: bfloat16 [2048, 256], P(None, 'tp'), may hold values from -8 to 8
- w_value: bfloat16 [2048, 256], P(None, 'tp'), may hold values from -0.125 to 0.125
- w_output: bfloat16 [1024, 2048], replicated, may hold values from -0.1875 to 0.1875
- mixer_post_gain: float32 [2048], replicated, may hold values from 0.1 to 1.9
- expert_input: bfloat16 [2048, 2048], P('ep'), may hold values from -6 to 6
- expert_ids: int32 [2048, 2], P('ep'), may hold values from 0 to 7, all different within a row; in each aligned block of 64 rows (0 to 63, 64 to 127, ...) at most 32 rows name the same one
- route_weight: float32 [2048, 2], P('ep'), may hold values from 0.1 to 1
- expert_gain: float32 [2048], replicated, may hold values from 0.1 to 1.9
- w_gate: bfloat16 [8, 2048, 3584], P('ep', None, 'tp'), may hold values from -0.125 to 0.125
- w_up: bfloat16 [8, 2048, 3584], P('ep', None, 'tp'), may hold values from -0.125 to 0.125
- w_down: bfloat16 [8, 3584, 2048], P('ep', 'tp'), may hold values from -0.09375 to 0.09375
- expert_post_gain: float32 [2048], replicated, may hold values from 0.1 to 1.9
Outputs:
- mixer_out: bfloat16 [4096, 2048], P(('ep', 'tp'))
- expert_out: bfloat16 [2048, 2048], P(('ep', 'tp'))
Inputs may be any that keep to these rules, and one draw needn't show every extreme that they name: `expert_ids`: in each aligned block of 64 tokens no expert is named by more than 32 of them. `log_forget_total`: each head's values never rise along the positions.
All inputs are finite; a program needn't handle non-finite values.
Results may differ from a plain program's by a relative error of at most 0.012.
The roundings to bfloat16 on the way count: a program that leaves them out, or rounds other values in their place, can miss the bound.
Values may be sent and summed in bfloat16 or wider, within the bound.
A program may use at most 128 MiB of HBM per device.

v0:
```python
import math
import jax
import jax.numpy as jnp
from jax import lax
from jax.sharding import PartitionSpec as P

HD = 64
TOP_K = 2
NEG_FILL = -1e30
NORM_EPS = 1e-06


def norm_rows(values_in, gain_vec):
    widened = values_in.astype(jnp.float32)
    return (
        widened
        * lax.rsqrt(jnp.mean(widened * widened, axis=-1, keepdims=True) + NORM_EPS)
        * gain_vec
    )


def unchanged(present_state):
    return present_state


def mixer_half(
    mixer_input, log_forget_total, mixer_gain, w_query, w_key, w_value, w_output, mixer_post_gain
):
    row_count = mixer_input.shape[0]
    offset = lax.axis_index("ep") * row_count
    head_local = w_query.shape[1] // HD
    kv_local = w_key.shape[1] // HD
    group_size = head_local // kv_local
    normed = norm_rows(mixer_input, mixer_gain).astype(jnp.bfloat16)
    queries = (
        jnp.dot(normed, w_query, preferred_element_type=jnp.float32)
        .astype(jnp.bfloat16)
        .reshape(row_count, kv_local, group_size, HD)
    )
    key_rows = (
        jnp.dot(normed, w_key, preferred_element_type=jnp.float32)
        .astype(jnp.bfloat16)
        .reshape(row_count, kv_local, HD)
    )
    value_rows = (
        jnp.dot(normed, w_value, preferred_element_type=jnp.float32)
        .astype(jnp.bfloat16)
        .reshape(row_count, kv_local, HD)
    )
    gate_totals = log_forget_total.reshape(kv_local, group_size, -1)
    query_gate = lax.dynamic_slice_in_dim(gate_totals, offset, row_count, 2)
    query_pos = offset + jnp.arange(row_count, dtype=jnp.int32)
    last_row = offset + row_count - 1
    score_scale = HD ** (-0.5)
    start_state = (
        jnp.full((kv_local, group_size, row_count), NEG_FILL, jnp.float32),
        jnp.zeros((kv_local, group_size, row_count), jnp.float32),
        jnp.zeros((kv_local, group_size, row_count, HD), jnp.float32),
    )
    running = start_state
    key_piece = lax.all_gather(key_rows, "ep", axis=0, tiled=True)
    value_piece = lax.all_gather(value_rows, "ep", axis=0, tiled=True)
    piece_rows = key_piece.shape[0]
    block_rows = math.gcd(piece_rows, 512)
    block_total = piece_rows // block_rows
    key_blocks = key_piece.reshape(block_total, block_rows, kv_local, HD)
    value_blocks = value_piece.reshape(block_total, block_rows, kv_local, HD)

    def one_block(present_state, operands):
        key_block, value_block, block_index = operands
        block_first = block_index * block_rows

        def update(prior_value):
            row_max, denominator, numerator = prior_value
            key_gate = lax.dynamic_slice_in_dim(gate_totals, block_first, block_rows, 2)
            scores = (
                jnp.einsum("qgjd,kgd->gjqk", queries, key_block, preferred_element_type=jnp.float32)
                * score_scale
            )
            scores = scores + query_gate[:, :, :, None] - key_gate[:, :, None, :]
            visible = (block_first + jnp.arange(block_rows, dtype=jnp.int32))[None, :] <= query_pos[
                :, None
            ]
            scores = jnp.where(visible, scores, NEG_FILL)
            new_max = jnp.maximum(row_max, jnp.max(scores, axis=-1))
            shifted = jnp.where(visible, jnp.exp(scores - new_max[..., None]), 0.0)
            factor = jnp.exp(row_max - new_max)
            denominator = denominator * factor + jnp.sum(shifted, axis=-1)
            numerator = numerator * factor[..., None] + jnp.einsum(
                "gjqk,kgd->gjqd",
                shifted.astype(jnp.bfloat16),
                value_block,
                preferred_element_type=jnp.float32,
            )
            return (new_max, denominator, numerator)

        return (lax.cond(block_first <= last_row, update, unchanged, present_state), None)

    running, _ = lax.scan(
        one_block, running, (key_blocks, value_blocks, jnp.arange(block_total, dtype=jnp.int32))
    )
    row_max, denominator, numerator = running
    mixed_heads = (
        jnp.transpose(numerator / denominator[..., None], (2, 0, 1, 3))
        .reshape(row_count, head_local * HD)
        .astype(jnp.bfloat16)
    )
    by_rows = lax.all_to_all(mixed_heads, "tp", split_axis=0, concat_axis=1, tiled=True)
    projected = jnp.dot(by_rows, w_output, preferred_element_type=jnp.float32)
    return norm_rows(projected, mixer_post_gain).astype(jnp.bfloat16)


def expert_half(
    expert_input, expert_ids, route_weight, expert_gain, w_gate, w_up, w_down, expert_post_gain
):
    row_count = expert_input.shape[0]
    quarters = lax.axis_size("tp")
    experts = lax.axis_size("ep")
    quarter_rows = row_count // quarters
    slot_count = 2 * TOP_K * quarter_rows // experts
    own_quarter = lax.axis_index("tp")
    normed = norm_rows(expert_input, expert_gain).astype(jnp.bfloat16)
    padded_rows = jnp.concatenate([normed, jnp.zeros((1, normed.shape[1]), jnp.bfloat16)], axis=0)
    routed = expert_ids.reshape(quarters, quarter_rows * TOP_K)
    matches = (routed[:, :, None] == jnp.arange(experts, dtype=jnp.int32)[None, None, :]).astype(
        jnp.int32
    )
    slot_ranks = jnp.sum(jnp.cumsum(matches, axis=1) * matches, axis=2) - 1
    owners = (jnp.arange(row_count * TOP_K, dtype=jnp.int32) // TOP_K).reshape(
        quarters, quarter_rows * TOP_K
    )
    quarter_index = jnp.broadcast_to(jnp.arange(quarters, dtype=jnp.int32)[:, None], routed.shape)
    slot_table = (
        jnp.full((quarters, slot_count, experts), row_count, jnp.int32)
        .at[quarter_index, slot_ranks, routed]
        .set(owners)
    )
    gate_local = w_gate[0]
    up_local = w_up[0]
    down_local = w_down[0]
    unit_count = gate_local.shape[1]
    own_table = lax.dynamic_index_in_dim(slot_table, own_quarter, 0, keepdims=False)
    outgoing = padded_rows[own_table]
    arrived = lax.all_to_all(outgoing, "ep", split_axis=1, concat_axis=1, tiled=True)
    slot_rows = lax.all_gather(arrived[None], "tp", axis=0, tiled=True)
    flat_rows = slot_rows.reshape(-1, slot_rows.shape[-1])
    gate_part = jnp.dot(flat_rows, gate_local, preferred_element_type=jnp.float32)
    up_part = jnp.dot(flat_rows, up_local, preferred_element_type=jnp.float32)
    hidden = (
        (jax.nn.silu(gate_part) * up_part)
        .astype(jnp.bfloat16)
        .reshape(slot_rows.shape[:-1] + (unit_count,))
    )
    product = jnp.dot(
        hidden.reshape(-1, unit_count), down_local, preferred_element_type=jnp.float32
    )
    summed = lax.psum_scatter(
        product.reshape(lax.axis_size("tp") * 1, slot_count, experts, product.shape[-1]).astype(
            jnp.bfloat16
        ),
        "tp",
        scatter_dimension=0,
        tiled=True,
    ).astype(jnp.float32)
    results = summed[0].astype(jnp.bfloat16)
    returned = lax.all_to_all(results, "ep", split_axis=1, concat_axis=1, tiled=True)
    flat_results = returned.reshape(slot_count * experts, returned.shape[-1])
    own_routes = lax.dynamic_index_in_dim(routed, own_quarter, 0, keepdims=False)
    own_ranks = lax.dynamic_index_in_dim(slot_ranks, own_quarter, 0, keepdims=False)
    picked = flat_results[own_ranks * experts + own_routes].reshape(quarter_rows, TOP_K, -1)
    own_weights = lax.dynamic_slice_in_dim(
        route_weight, own_quarter * quarter_rows, quarter_rows, 0
    )
    combined = jnp.sum(own_weights[:, :, None] * picked.astype(jnp.float32), axis=1)
    return norm_rows(combined, expert_post_gain).astype(jnp.bfloat16)


def per_device(
    mixer_input,
    log_forget_total,
    mixer_gain,
    w_query,
    w_key,
    w_value,
    w_output,
    mixer_post_gain,
    expert_input,
    expert_ids,
    route_weight,
    expert_gain,
    w_gate,
    w_up,
    w_down,
    expert_post_gain,
):
    mixer_out = mixer_half(
        mixer_input,
        log_forget_total,
        mixer_gain,
        w_query,
        w_key,
        w_value,
        w_output,
        mixer_post_gain,
    )
    expert_out = expert_half(
        expert_input, expert_ids, route_weight, expert_gain, w_gate, w_up, w_down, expert_post_gain
    )
    return (mixer_out, expert_out)


def solution(mesh):
    placed = (
        P("ep", None),
        P("tp", None),
        P(),
        P(None, "tp"),
        P(None, "tp"),
        P(None, "tp"),
        P(),
        P(),
        P("ep", None),
        P("ep", None),
        P("ep", None),
        P(),
        P("ep", None, "tp"),
        P("ep", None, "tp"),
        P("ep", "tp", None),
        P(),
    )
    return jax.shard_map(
        per_device,
        mesh=mesh,
        in_specs=placed,
        out_specs=(P(("ep", "tp"), None), P(("ep", "tp"), None)),
        check_vma=False,
    )
```

profile of v0, /device:TPU:0, one launch (start us, length us, event | category | flops | bytes accessed | tf_op | source)
XLA Modules:
  0.0 324.2 jit_solution(3863174267052389493)
XLA Ops:
  7.2 0.9 copy.41
  8.2 0.1 eq.15
  8.3 0.1 reshape.284
  8.5 0.1 fusion.46
  8.7 0.3 reduce_window_sum.11
  8.9 0.2 select_reduce_fusion
  9.2 29.5 %scatter_fusion = s32[4,32,8]{1,2,0:T(8,128)S(1)} fusion(s32[4,32,8]{1,2,0:T(8,128)S(1)} %broadcast_in_dim.39, s32[512]{0:T(512)S(1)} %fusion.52, s32[512]{0:T(512)S(1)} %fusion.54), kind=kCustom, calls=%fused_computation.2 | custom fusion | bytes 12288 | tf_op jit(solution)/shard_map/scatter | solution.py:136
  38.8 0.1 copy.43
  38.8 0.1 reshape.290
  39.0 0.3 fusion.43
  39.3 0.3 fusion.45
  39.6 0.1 concatenate.6
  39.7 1.4 gather_fusion
  41.0 0.6 copy.44
  41.6 32.9 %all_to_all.26 = bf16[32,8,2048]{2,0,1:T(8,128)(2,1)S(1)} all-to-all(bf16[32,8,2048]{2,0,1:T(8,128)(2,1)S(1)} %copy.44), channel_id=1, replica_groups=mesh['ep'=8,'tp'=4] {'ep'}, dimensions={1} | all-to-all | bytes 2097152 | tf_op jit(solution)/shard_map/all_to_all | solution.py:144
  74.5 1.6 copy.45
  76.1 0.2 reduce-scatter.2.cloned.1.call-start
  76.3 33.4 %all-gather.5.cloned.1.call-done = bf16[128,8,2048]{2,1,0:T(8,128)(2,1)} async-done(((bf16[32,8,2048]{2,1,0:T(8,128)(2,1)}), bf16[128,8,2048]{2,1,0:T(8,128)(2,1)}) %all-gather.5.cloned.1.call-update) | async-done | bytes 4194320 | tf_op jit(solution)/shard_map/all_gather | solution.py:145
  109.7 7.5 %fusion.32 = f32[1024,896]{1,0:T(8,128)S(1)} fusion(bf16[128,8,2048]{2,1,0:T(8,128)(2,1)} %all-gather.5.cloned.1.call-done, bf16[1,2048,896]{2,1,0:T(8,128)(2,1)} %param.33), kind=kOutput, calls=%fused_computation.40 | convolution fusion | flops 3758096384 | bytes 11534336 | tf_op jit(solution)/shard_map/dot_general | solution.py:148
  117.2 4.8 %multiply_convert_fusion = bf16[1024,896]{1,0:T(8,128)(2,1)S(1)} fusion(f32[1024,896]{1,0:T(8,128)S(1)} %fusion.32, bf16[1,2048,896]{2,1,0:T(8,128)(2,1)S(1)} %copy-done.11, bf16[128,8,2048]{2,1,0:T(8,128)(2,1)S(1)} %copy-done.10), kind=kOutput, calls=%fused_computation.48 | convolution fusion | flops 3763601408 | bytes 13369344 | tf_op jit(solution)/shard_map/dot_general | solution.py:147
  122.0 6.0 %convolution_convert_fusion = bf16[4,32,8,2048]{3,2,1,0:T(8,128)(2,1)} fusion(bf16[4,32,8,896]{3,2,1,0:T(8,128)(2,1)S(1)} %bitcast.163, bf16[1,896,2048]{2,1,0:T(8,128)(2,1)S(1)} %copy-done.12), kind=kOutput, calls=%fused_computation.44 | convolution fusion | flops 3760193536 | bytes 9699328 | tf_op jit(solution)/shard_map/dot_general | solution.py:154
  128.0 1.5 copy-done.1
  129.6 0.5 fusion.29
  130.1 2.2 fusion.31
  132.3 0.8 convolution_convert_fusion.3
  133.0 31.5 %all-gather = bf16[4096,64]{0,1:T(8,128)(2,1)S(1)} all-gather(bf16[512,64]{0,1:T(8,128)(2,1)S(1)} %convolution_convert_fusion.3), channel_id=2, replica_groups=mesh['ep'=8,'tp'=4] {'ep'}, dimensions={0}, use_global_device_ids=true | all-gather | bytes 589824 | tf_op jit(solution)/shard_map/all_gather | solution.py:61
  164.5 0.2 copy.50
  164.7 0.9 copy.37
  165.6 0.8 convolution_convert_fusion.2
  166.4 31.4 %all-gather.1 = bf16[4096,64]{0,1:T(8,128)(2,1)S(1)} all-gather(bf16[512,64]{0,1:T(8,128)(2,1)S(1)} %convolution_convert_fusion.2), channel_id=3, replica_groups=mesh['ep'=8,'tp'=4] {'ep'}, dimensions={0}, use_global_device_ids=true | all-gather | bytes 589824 | tf_op jit(solution)/shard_map/all_gather | solution.py:62
  197.8 0.2 copy.51
  198.0 1.0 copy.38
  199.0 0.7 dynamic-slice_bitcast_fusion.1
  199.7 1.5 convolution_convert_fusion.1
  201.2 18.1 %while.15 = (s32[]{:T(128)}, f32[1,4,512]{2,1,0:T(4,128)S(1)}, f32[1,4,512]{2,1,0:T(4,128)S(1)}, f32[1,4,512,64]{2,3,1,0:T(8,128)S(1)}, s32[8]{0:T(128)S(1)}, /*...) while((s32[]{:T(128)}, f32[1,4,512]{2,1,0:T(4,128)S(1)}, ...), condition=%wide.region_6.7_spmd.clone, body=%wide.region_1.6_spmd.clone.sunk | while | flops 288889856 | bytes 15283569 | solution.py:99
  201.2 0.7 dynamic_slice.79
  202.5 7.4 %conditional.3 = ((f32[1,4,512]{2,1,0:T(4,128)S(1)}, f32[1,4,512]{2,1,0:T(4,128)S(1)}, f32[1,4,512,64]{2,3,1,0:T(8,128)S(1)})) conditional(s32[]{:T(128)} %convert_element_type.123, (f32[1,4,512]{2,1,0:T(4,128)S(1)}, f32[1,4,512]{2,1,0:T(4,128)S(1)}, f32[1,4,512,64]{2,3,1,0:T(8,128)S(1)}) %tuple.48, (s32[]{:T(128)}, s32[]{:T(128)}, ...), branch_computations={%region_2.2_spmd, %region_3.5_spmd} | conditional | flops 288889856 | bytes 15281230 | solution.py:97
  202.5 0.8 dynamic-slice_bitcast_fusion
  203.3 0.2 broadcast_compare_fusion
  203.6 2.2 fusion.6
  205.8 2.6 fusion.14
  208.4 1.5 fusion.5
  210.0 0.7 dynamic_slice.79
  211.3 0.7 dynamic_slice.79
  212.6 0.7 dynamic_slice.79
  214.0 0.7 dynamic_slice.79
  215.3 0.7 dynamic_slice.79
  216.7 0.7 dynamic_slice.79
  218.0 0.7 dynamic_slice.79
  219.5 0.7 copy.39
  220.2 3.4 %all-to-all-start = ((bf16[4,128,256]{1,2,0:T(8,128)(2,1)}), bf16[4,128,256]{1,2,0:T(8,128)(2,1)S(1)}, u32[]{:S(2)}, u32[]{:S(2)}) async-start(bf16[4,128,256]{1,2,0:T(8,128)(2,1)} %copy.39), calls=%async_computation | async-start | bytes 524288 | tf_op jit(solution)/shard_map/all_to_all | solution.py:108
  223.7 2.8 copy.46
  226.5 3.1 all-to-all-done
  229.6 57.5 %all-to-all-start.2 = ((bf16[32,8,2048]{2,0,1:T(8,128)(2,1)}), bf16[32,8,2048]{2,0,1:T(8,128)(2,1)S(1)}, u32[]{:S(2)}, u32[]{:S(2)}) async-start(bf16[32,8,2048]{2,0,1:T(8,128)(2,1)} %copy.46), calls=%async_computation.3 | async-start | bytes 2097152 | tf_op jit(solution)/shard_map/all_to_all | solution.py:166
  287.2 0.1 copy.40
  287.3 3.0 multiply_reduce_fusion.1
  290.3 1.0 multiply_convert_fusion.1
  291.3 21.4 %all-to-all-done.2 = bf16[32,8,2048]{2,0,1:T(8,128)(2,1)S(1)} async-done(((bf16[32,8,2048]{2,0,1:T(8,128)(2,1)}), bf16[32,8,2048]{2,0,1:T(8,128)(2,1)S(1)}, u32[]{:S(2)}, u32[]{:S(2)}) %all-to-all-start.2) | async-done | bytes 1048608 | tf_op jit(solution)/shard_map/all_to_all | solution.py:166
  312.7 0.6 copy.53
  313.3 0.9 gather_fusion.1
  314.2 0.7 reshape.287
  314.9 1.5 multiply_reduce_fusion
  316.4 0.1 multiply_reduce_fusion.2
  316.6 0.8 multiply_convert_fusion.2
  (67 shorter events, 0.6 us)
Async XLA Ops:
  7.2 192.5 %copy-start = (bf16[2048,256]{1,0:T(8,128)(2,1)S(1)}, bf16[2048,256]{1,0:T(8,128)(2,1)}, u32[]{:S(2)}) copy-start(bf16[2048,256]{1,0:T(8,128)(2,1)} %param.23) | copy-start | bytes 3145732
  7.2 31.8 %copy-start.2 = (bf16[256,2048]{1,0:T(8,128)(2,1)S(1)}, bf16[256,2048]{1,0:T(8,128)(2,1)}, u32[]{:S(2)}) copy-start(bf16[256,2048]{1,0:T(8,128)(2,1)} %param.28) | copy-start | bytes 3145732
  7.2 32.1 %copy-start.5 = (f32[2048]{0:T(1024)S(1)}, f32[2048]{0:T(1024)}, u32[]{:S(2)}) copy-start(f32[2048]{0:T(1024)} %param.31) | copy-start | bytes 24580
  7.2 102.5 %all-gather.5.cloned.1.call-start = ((), (), s32[]{:S(2)}) async-start(), calls=%async_computation.5 | async-start | bytes 5242880 | tf_op jit(solution)/shard_map/all_gather | solution.py:145
  76.1 147.6 %reduce-scatter.2.cloned.1.call-start = ((), (), s32[]{:S(2)}) async-start(), calls=%async_computation.4 | async-start | bytes 5242880 | tf_op jit(solution)/shard_map/reduce_scatter | solution.py:157
  109.7 7.5 %copy-start.10 = (bf16[128,8,2048]{2,1,0:T(8,128)(2,1)S(1)}, bf16[128,8,2048]{2,1,0:T(8,128)(2,1)}, u32[]{:S(2)}) copy-start(bf16[128,8,2048]{2,1,0:T(8,128)(2,1)} %all-gather.5.cloned.1.call-done) | copy-start | bytes 12582916
  109.7 7.5 %copy-start.11 = (bf16[1,2048,896]{2,1,0:T(8,128)(2,1)S(1)}, bf16[1,2048,896]{2,1,0:T(8,128)(2,1)}, u32[]{:S(2)}) copy-start(bf16[1,2048,896]{2,1,0:T(8,128)(2,1)} %param.32) | copy-start | bytes 11010052
  117.2 4.8 %copy-start.12 = (bf16[1,896,2048]{2,1,0:T(8,128)(2,1)S(1)}, bf16[1,896,2048]{2,1,0:T(8,128)(2,1)}, u32[]{:S(2)}) copy-start(bf16[1,896,2048]{2,1,0:T(8,128)(2,1)} %param.34) | copy-start | bytes 11010052
  128.0 1.6 copy-start.1
  128.0 2.1 copy-start.6
  128.0 4.3 %copy-start.3 = (bf16[2048,64]{0,1:T(8,128)(2,1)S(1)}, bf16[2048,64]{0,1:T(8,128)(2,1)}, u32[]{:S(2)}) copy-start(bf16[2048,64]{0,1:T(8,128)(2,1)} %param.24) | copy-start | bytes 786436
  130.1 35.5 %copy-start.4 = (bf16[2048,64]{0,1:T(8,128)(2,1)S(1)}, bf16[2048,64]{0,1:T(8,128)(2,1)}, u32[]{:S(2)}) copy-start(bf16[2048,64]{0,1:T(8,128)(2,1)} %param.25) | copy-start | bytes 786436
  219.4 67.7 %copy-start.9 = (f32[256,2]{0,1:T(2,128)S(1)}, f32[256,2]{0,1:T(2,128)}, u32[]{:S(2)}) copy-start(f32[256,2]{0,1:T(2,128)} %param.30) | copy-start | bytes 6148
  220.2 9.4 %all-to-all-start = ((bf16[4,128,256]{1,2,0:T(8,128)(2,1)}), bf16[4,128,256]{1,2,0:T(8,128)(2,1)S(1)}, u32[]{:S(2)}, u32[]{:S(2)}) async-start(bf16[4,128,256]{1,2,0:T(8,128)(2,1)} %copy.39), calls=%async_computation | async-start | bytes 524288 | tf_op jit(solution)/shard_map/all_to_all | solution.py:108
  226.5 63.9 %copy-start.7 = (f32[2048]{0:T(1024)S(1)}, f32[2048]{0:T(1024)}, u32[]{:S(2)}) copy-start(f32[2048]{0:T(1024)} %param.27) | copy-start | bytes 24580
  229.6 83.1 %all-to-all-start.2 = ((bf16[32,8,2048]{2,0,1:T(8,128)(2,1)}), bf16[32,8,2048]{2,0,1:T(8,128)(2,1)S(1)}, u32[]{:S(2)}, u32[]{:S(2)}) async-start(bf16[32,8,2048]{2,0,1:T(8,128)(2,1)} %copy.46), calls=%async_computation.3 | async-start | bytes 2097152 | tf_op jit(solution)/shard_map/all_to_all | solution.py:166
  313.3 3.3 %copy-start.8 = (f32[2048]{0:T(1024)S(1)}, f32[2048]{0:T(1024)}, u32[]{:S(2)}) copy-start(f32[2048]{0:T(1024)} %param.35) | copy-start | bytes 24580
Sparse Core Ops, SparseCore 0:
  76.2 33.4 all-gather.4
  128.1 44.5 reduce-scatter.1
where the time goes:
time: 326 us; the launch traced here: 324 us
  blocking collectives  95.8 us (29%)
  starting transfers between devices  61.1 us (19%)
  waiting for transfers between devices  58 us (18%)
  local copies, waits for them, and re-layouts  51.1 us (16%)
  matrix products  29 us (9%)
  between operations  14.4 us (4%)
  other arithmetic  9.24 us (3%)
  loops' own time  5.57 us (2%)
    all_to_all x1, starting transfers between devices, expert_half(): lax.all_to_all(results, 'ep', split_axis=1, concat_axis=1, tiled=True)  57.5 us
    all_gather x1, waiting for transfers between devices, expert_half(): slot_rows = lax.all_gather(arrived[None], 'tp', axis=0, tiled=True)  33.4 us
    all_to_all x1, blocking collectives, expert_half(): lax.all_to_all(outgoing, 'ep', split_axis=1, concat_axis=1, tiled=True)  32.9 us
    all_gather x1, blocking collectives, mixer_half(): key_piece = lax.all_gather(key_rows, 'ep', axis=0, tiled=True)  31.5 us
    all_gather x1, blocking collectives, mixer_half(): value_piece = lax.all_gather(value_rows, 'ep', axis=0, tiled=True)  31.4 us
    scatter x1, local copies, waits for them, and re-layouts, expert_half(): slot_table = jnp.full((quarters, slot_count, experts), row_count, jnp.int...  29.5 us
    all_to_all x1, waiting for transfers between devices, expert_half(): lax.all_to_all(results, 'ep', split_axis=1, concat_axis=1, tiled=True)  21.4 us
    dot_general x1, matrix products, expert_half(): up_part = jnp.dot(flat_rows, up_local, preferred_element_type=jnp.float32)  7.49 us
  transfers between devices with their start and end apart: 4, of which 3 were waited for; matrix products, arithmetic and copies ran while one was open for 9% of the time, Pallas kernels for 0%

commit v1 on v0

--- a/solution.py
+++ b/solution.py
@@ -3,6 +3,7 @@
 import jax.numpy as jnp
 from jax import lax
 from jax.sharding import PartitionSpec as P
+from jax.lax import all_gather
 
 HD = 64
 TOP_K = 2
@@ -58,8 +59,13 @@
         jnp.zeros((kv_local, group_size, row_count, HD), jnp.float32),
     )
     running = start_state
-    key_piece = lax.all_gather(key_rows, "ep", axis=0, tiled=True)
-    value_piece = lax.all_gather(value_rows, "ep", axis=0, tiled=True)
+    key_piece, value_piece = jnp.split(
+        all_gather(
+            jnp.concatenate([key_rows, value_rows], axis=1), axis_name="ep", axis=0, tiled=True
+        ),
+        [key_rows.shape[1]],
+        axis=1,
+    )
     piece_rows = key_piece.shape[0]
     block_rows = math.gcd(piece_rows, 512)
     block_total = piece_rows // block_rows

time: 326 us -> 262 us (0.80)
  blocking collectives: 95.8 us -> 32.9 us
  waiting for transfers between devices: 58 us -> 98.5 us
  starting transfers between devices: 61.1 us -> 22.1 us
    all_gather x2 -> x0, blocking collectives: 62.9 us -> none  [the longest x1 31.5 us: mixer_half(): key_piece = lax.all_gather(key_rows, 'ep', axis=0, tiled=True)]
    all_to_all x1, starting transfers between devices: 57.5 us -> 18.2 us  [expert_half(): lax.all_to_all(results, 'ep', split_axis=1, concat_axis=1, tiled=True)]
    reduce_scatter x1, waiting for transfers between devices: 0.02 us -> 27 us  [expert_half(): lax.psum_scatter(product.reshape(lax.axis_size('tp') * 1, slot_count, exp...]
    all_gather x0 -> x1, waiting for transfers between devices: none -> 21.6 us  [mixer_half(): all_gather(jnp.concatenate([key_rows, value_rows], axis=1), axis_name='ep...]
    all_gather x1, waiting for transfers between devices: 33.4 us -> 28.4 us  [expert_half(): slot_rows = lax.all_gather(arrived[None], 'tp', axis=0, tiled=True)]
    unnamed x31 -> x30, local copies, waits for them, and re-layouts: 4.81 us -> 1.12 us
  transfers between devices with their start and end apart: 4 -> 5, of which waited for: 3 -> 4; matrix products, arithmetic and copies ran while one was open for 9% -> 17% of each run, Pallas kernels for 0% -> 0%
where the time goes in v1:
time: 262 us; the launch traced here: 261 us
  waiting for transfers between devices  98.5 us (38%)
  local copies, waits for them, and re-layouts  50.5 us (19%)
  blocking collectives  32.9 us (13%)
  matrix products  27.2 us (10%)
  starting transfers between devices  22.1 us (8%)
  between operations  14.1 us (5%)
  other arithmetic  9.88 us (4%)
  loops' own time  5.7 us (2%)
    all_to_all x1, blocking collectives, expert_half(): lax.all_to_all(outgoing, 'ep', split_axis=1, concat_axis=1, tiled=True)  32.9 us
    scatter x1, local copies, waits for them, and re-layouts, expert_half(): slot_table = jnp.full((quarters, slot_count, experts), row_count, jnp.int...  29.5 us
    all_gather x1, waiting for transfers between devices, expert_half(): slot_rows = lax.all_gather(arrived[None], 'tp', axis=0, tiled=True)  28.4 us
    reduce_scatter x1, waiting for transfers between devices, expert_half(): lax.psum_scatter(product.reshape(lax.axis_size('tp') * 1, slot_count, exp...  27 us
    all_gather x1, waiting for transfers between devices, mixer_half(): all_gather(jnp.concatenate([key_rows, value_rows], axis=1), axis_name='ep...  21.6 us
    all_to_all x1, waiting for transfers between devices, expert_half(): lax.all_to_all(results, 'ep', split_axis=1, concat_axis=1, tiled=True)  21.4 us
    all_to_all x1, starting transfers between devices, expert_half(): lax.all_to_all(results, 'ep', split_axis=1, concat_axis=1, tiled=True)  18.2 us
    dot_general x1, matrix products, expert_half(): up_part = jnp.dot(flat_rows, up_local, preferred_element_type=jnp.float32)  7.49 us
  transfers between devices with their start and end apart: 5, of which 4 were waited for; matrix products, arithmetic and copies ran while one was open for 17% of the time, Pallas kernels for 0%

profile of v1, /device:TPU:0, one launch (start us, length us, event | category | flops | bytes accessed | tf_op | source)
XLA Modules:
  0.0 260.8 jit_solution(5046767718479833160)
XLA Ops:
  7.2 0.9 copy.41
  8.2 0.1 eq.15
  8.3 0.1 reshape.284
  8.5 0.1 fusion.48
  8.7 0.3 reduce_window_sum.11
  8.9 0.2 select_reduce_fusion
  9.2 29.5 %scatter_fusion = s32[4,32,8]{1,2,0:T(8,128)S(1)} fusion(s32[4,32,8]{1,2,0:T(8,128)S(1)} %broadcast_in_dim.39, s32[512]{0:T(512)S(1)} %fusion.54, s32[512]{0:T(512)S(1)} %fusion.56), kind=kCustom, calls=%fused_computation.2 | custom fusion | bytes 12288 | tf_op jit(solution)/shard_map/scatter | solution.py:142
  38.8 0.1 copy.43
  38.8 0.1 reshape.290
  39.0 0.3 fusion.43
  39.3 0.3 fusion.45
  39.6 0.1 concatenate.10
  39.7 2.3 gather_fusion
  42.0 2.0 copy.44
  44.0 32.9 %all_to_all.26 = bf16[32,8,2048]{2,0,1:T(8,128)(2,1)S(1)} all-to-all(bf16[32,8,2048]{2,0,1:T(8,128)(2,1)S(1)} %copy.44), channel_id=1, replica_groups=mesh['ep'=8,'tp'=4] {'ep'}, dimensions={1} | all-to-all | bytes 2097152 | tf_op jit(solution)/shard_map/all_to_all | solution.py:150
  76.8 1.6 copy.45
  78.5 0.5 fusion.29
  79.0 2.1 fusion.31
  81.1 0.8 fusion.46
  81.9 0.8 fusion.47
  82.7 0.7 pad_maximum_fusion
  83.4 0.2 reduce-scatter.2.cloned.1.call-start
  83.6 28.4 %all-gather.6.cloned.1.call-done = bf16[128,8,2048]{2,1,0:T(8,128)(2,1)} async-done(((bf16[32,8,2048]{2,1,0:T(8,128)(2,1)}), bf16[128,8,2048]{2,1,0:T(8,128)(2,1)}) %all-gather.6.cloned.1.call-update) | async-done | bytes 4194320 | tf_op jit(solution)/shard_map/all_gather | solution.py:151
  112.0 7.5 %fusion.32 = f32[1024,896]{1,0:T(8,128)S(1)} fusion(bf16[128,8,2048]{2,1,0:T(8,128)(2,1)} %all-gather.6.cloned.1.call-done, bf16[1,2048,896]{2,1,0:T(8,128)(2,1)} %param.33), kind=kOutput, calls=%fused_computation.40 | convolution fusion | flops 3758096384 | bytes 11534336 | tf_op jit(solution)/shard_map/dot_general | solution.py:154
  119.6 4.8 %multiply_convert_fusion = bf16[1024,896]{1,0:T(8,128)(2,1)S(1)} fusion(f32[1024,896]{1,0:T(8,128)S(1)} %fusion.32, bf16[1,2048,896]{2,1,0:T(8,128)(2,1)S(1)} %copy-done.11, bf16[128,8,2048]{2,1,0:T(8,128)(2,1)S(1)} %copy-done.10), kind=kOutput, calls=%fused_computation.48 | convolution fusion | flops 3763601408 | bytes 13369344 | tf_op jit(solution)/shard_map/dot_general | solution.py:153
  124.3 6.0 %convolution_convert_fusion = bf16[4,32,8,2048]{3,2,1,0:T(8,128)(2,1)} fusion(bf16[4,32,8,896]{3,2,1,0:T(8,128)(2,1)S(1)} %bitcast.161, bf16[1,896,2048]{2,1,0:T(8,128)(2,1)S(1)} %copy-done.12), kind=kOutput, calls=%fused_computation.44 | convolution fusion | flops 3760193536 | bytes 9699328 | tf_op jit(solution)/shard_map/dot_general | solution.py:160
  130.4 0.7 dynamic-slice_bitcast_fusion.1
  131.1 1.5 convolution_convert_fusion.1
  132.5 21.6 %all-gather.4.cloned.1.call-done = bf16[4096,2,64]{0,2,1:T(8,128)(2,1)} async-done(((bf16[512,2,64]{0,2,1:T(8,128)(2,1)}), bf16[4096,2,64]{0,2,1:T(8,128)(2,1)}) %all-gather.4.cloned.1.call-update) | async-done | bytes 1048592 | tf_op jit(solution)/shard_map/all_gather | solution.py:63
  154.1 1.3 fusion.65
  155.4 0.1 copy_bitcast_fusion.1
  155.6 15.9 %while.15 = (s32[]{:T(128)}, f32[1,4,512]{2,1,0:T(4,128)S(1)}, f32[1,4,512]{2,1,0:T(4,128)S(1)}, f32[1,4,512,64]{2,3,1,0:T(8,128)S(1)}, s32[8]{0:T(128)S(1)}, /*...) while((s32[]{:T(128)}, f32[1,4,512]{2,1,0:T(4,128)S(1)}, ...), condition=%wide.region_6.7_spmd.clone, body=%wide.region_1.6_spmd.clone.sunk | while | flops 288889856 | bytes 15282553 | solution.py:105
  155.6 0.6 dynamic_slice.79
  156.9 5.6 %conditional.3 = ((f32[1,4,512]{2,1,0:T(4,128)S(1)}, f32[1,4,512]{2,1,0:T(4,128)S(1)}, f32[1,4,512,64]{2,3,1,0:T(8,128)S(1)})) conditional(s32[]{:T(128)} %convert_element_type.127, (f32[1,4,512]{2,1,0:T(4,128)S(1)}, f32[1,4,512]{2,1,0:T(4,128)S(1)}, f32[1,4,512,64]{2,3,1,0:T(8,128)S(1)}) %tuple.50, (s32[]{:T(128)}, s32[]{:T(128)}, ...), branch_computations={%region_2.2_spmd, %region_3.5_spmd} | conditional | flops 288889856 | bytes 15280214 | solution.py:103
  156.9 0.8 dynamic-slice_bitcast_fusion
  157.7 0.2 broadcast_compare_fusion
  157.9 1.2 fusion.6
  159.1 1.7 fusion.14
  160.9 1.5 fusion.5
  162.4 0.6 dynamic_slice.79
  163.7 0.6 dynamic_slice.79
  165.0 0.6 dynamic_slice.79
  166.3 0.6 dynamic_slice.79
  167.6 0.6 dynamic_slice.79
  168.9 0.6 dynamic_slice.79
  170.2 0.6 dynamic_slice.79
  171.5 0.1 fusion.49
  171.6 0.1 convert_element_type.72
  171.6 0.7 copy.39
  172.4 3.6 %all-to-all-start = ((bf16[4,128,256]{1,2,0:T(8,128)(2,1)}), bf16[4,128,256]{1,2,0:T(8,128)(2,1)S(1)}, u32[]{:S(2)}, u32[]{:S(2)}) async-start(bf16[4,128,256]{1,2,0:T(8,128)(2,1)} %copy.39), calls=%async_computation | async-start | bytes 524288 | tf_op jit(solution)/shard_map/all_to_all | solution.py:114
  176.0 27.0 %reduce-scatter.2.cloned.1.call-done = bf16[1,32,8,2048]{3,2,1,0:T(8,128)(2,1)} async-done(((bf16[4,32,8,2048]{3,2,1,0:T(8,128)(2,1)}), bf16[1,32,8,2048]{3,2,1,0:T(8,128)(2,1)}) %reduce-scatter.2.cloned.1.call-update) | async-done | bytes 1048592 | tf_op jit(solution)/shard_map/reduce_scatter | solution.py:163
  203.1 2.8 %copy.46 = bf16[32,8,2048]{2,0,1:T(8,128)(2,1)} copy(bf16[32,8,2048]{2,1,0:T(8,128)(2,1)} %bitcast.155) | data formatting | bytes 2097152 | tf_op jit(solution)/shard_map/convert_element_type | solution.py:171
  205.8 18.2 %all-to-all-start.2 = ((bf16[32,8,2048]{2,0,1:T(8,128)(2,1)}), bf16[32,8,2048]{2,0,1:T(8,128)(2,1)S(1)}, u32[]{:S(2)}, u32[]{:S(2)}) async-start(bf16[32,8,2048]{2,0,1:T(8,128)(2,1)} %copy.46), calls=%async_computation.3 | async-start | bytes 2097152 | tf_op jit(solution)/shard_map/all_to_all | solution.py:172
  224.0 0.1 constant_dynamic-slice_fusion.2
  224.1 0.1 copy.40
  224.2 3.0 %multiply_reduce_fusion.1 = (f32[128]{0:T(128)S(1)}, f32[128,2048]{1,0:T(8,128)S(1)}) fusion(bf16[128,1024]{0,1:T(8,128)(2,1)S(1)} %bitcast.154, bf16[1024,2048]{1,0:T(8,128)(2,1)} %param.26), kind=kOutput, calls=%fused_computation.62 | convolution fusion | flops 537395072 | bytes 5505536 | tf_op jit(solution)/shard_map/dot_general | solution.py:115
  227.2 1.0 multiply_convert_fusion.1
  228.2 21.4 %all-to-all-done.2 = bf16[32,8,2048]{2,0,1:T(8,128)(2,1)S(1)} async-done(((bf16[32,8,2048]{2,0,1:T(8,128)(2,1)}), bf16[32,8,2048]{2,0,1:T(8,128)(2,1)S(1)}, u32[]{:S(2)}, u32[]{:S(2)}) %all-to-all-start.2) | async-done | bytes 1048608 | tf_op jit(solution)/shard_map/all_to_all | solution.py:172
  249.6 0.6 copy.55
  250.2 0.9 gather_fusion.1
  251.1 0.7 reshape.287
  251.8 1.5 multiply_reduce_fusion
  253.3 0.1 multiply_reduce_fusion.2
  253.5 0.8 multiply_convert_fusion.2
  (69 shorter events, 0.5 us)
Async XLA Ops:
  7.2 123.9 %copy-start = (bf16[2048,256]{1,0:T(8,128)(2,1)S(1)}, bf16[2048,256]{1,0:T(8,128)(2,1)}, u32[]{:S(2)}) copy-start(bf16[2048,256]{1,0:T(8,128)(2,1)} %param.23) | copy-start | bytes 3145732
  7.2 31.8 %copy-start.2 = (bf16[256,2048]{1,0:T(8,128)(2,1)S(1)}, bf16[256,2048]{1,0:T(8,128)(2,1)}, u32[]{:S(2)}) copy-start(bf16[256,2048]{1,0:T(8,128)(2,1)} %param.28) | copy-start | bytes 3145732
  7.2 32.1 %copy-start.5 = (f32[2048]{0:T(1024)S(1)}, f32[2048]{0:T(1024)}, u32[]{:S(2)}) copy-start(f32[2048]{0:T(1024)} %param.31) | copy-start | bytes 24580
  7.2 104.8 %all-gather.6.cloned.1.call-start = ((), (), s32[]{:S(2)}) async-start(), calls=%async_computation.6 | async-start | bytes 5242880 | tf_op jit(solution)/shard_map/all_gather | solution.py:151
  42.0 36.5 %copy-start.1 = (bf16[512,2048]{1,0:T(8,128)(2,1)S(1)}, bf16[512,2048]{1,0:T(8,128)(2,1)}, u32[]{:S(2)}) copy-start(bf16[512,2048]{1,0:T(8,128)(2,1)} %param.20) | copy-start | bytes 6291460
  44.0 35.0 %copy-start.6 = (f32[2048]{0:T(1024)S(1)}, f32[2048]{0:T(1024)}, u32[]{:S(2)}) copy-start(f32[2048]{0:T(1024)} %param.22) | copy-start | bytes 24580
  78.4 2.7 %copy-start.3 = (bf16[2048,64]{0,1:T(8,128)(2,1)S(1)}, bf16[2048,64]{0,1:T(8,128)(2,1)}, u32[]{:S(2)}) copy-start(bf16[2048,64]{0,1:T(8,128)(2,1)} %param.24) | copy-start | bytes 786436
  78.4 75.7 %all-gather.4.cloned.1.call-start = ((), (), s32[]{:S(2)}) async-start(), calls=%async_computation.4 | async-start | bytes 1179648 | tf_op jit(solution)/shard_map/all_gather | solution.py:63
  78.5 3.4 %copy-start.4 = (bf16[2048,64]{0,1:T(8,128)(2,1)S(1)}, bf16[2048,64]{0,1:T(8,128)(2,1)}, u32[]{:S(2)}) copy-start(bf16[2048,64]{0,1:T(8,128)(2,1)} %param.25) | copy-start | bytes 786436
  83.4 119.7 %reduce-scatter.2.cloned.1.call-start = ((), (), s32[]{:S(2)}) async-start(), calls=%async_computation.5 | async-start | bytes 5242880 | tf_op jit(solution)/shard_map/reduce_scatter | solution.py:163
  112.0 7.5 %copy-start.10 = (bf16[128,8,2048]{2,1,0:T(8,128)(2,1)S(1)}, bf16[128,8,2048]{2,1,0:T(8,128)(2,1)}, u32[]{:S(2)}) copy-start(bf16[128,8,2048]{2,1,0:T(8,128)(2,1)} %all-gather.6.cloned.1.call-done) | copy-start | bytes 12582916
  112.0 7.5 %copy-start.11 = (bf16[1,2048,896]{2,1,0:T(8,128)(2,1)S(1)}, bf16[1,2048,896]{2,1,0:T(8,128)(2,1)}, u32[]{:S(2)}) copy-start(bf16[1,2048,896]{2,1,0:T(8,128)(2,1)} %param.32) | copy-start | bytes 11010052
  119.6 4.8 %copy-start.12 = (bf16[1,896,2048]{2,1,0:T(8,128)(2,1)S(1)}, bf16[1,896,2048]{2,1,0:T(8,128)(2,1)}, u32[]{:S(2)}) copy-start(bf16[1,896,2048]{2,1,0:T(8,128)(2,1)} %param.34) | copy-start | bytes 11010052
  132.5 23.0 %copy-start.13 = (bf16[512,256]{0,1:T(8,128)(2,1)S(1)}, bf16[512,256]{0,1:T(8,128)(2,1)}, u32[]{:S(2)}) copy-start(bf16[512,256]{0,1:T(8,128)(2,1)} %convolution_convert_fusion.1) | copy-start | bytes 786436
  171.5 52.5 %copy-start.9 = (f32[256,2]{0,1:T(2,128)S(1)}, f32[256,2]{0,1:T(2,128)}, u32[]{:S(2)}) copy-start(f32[256,2]{0,1:T(2,128)} %param.30) | copy-start | bytes 6148
  172.4 33.5 %all-to-all-start = ((bf16[4,128,256]{1,2,0:T(8,128)(2,1)}), bf16[4,128,256]{1,2,0:T(8,128)(2,1)S(1)}, u32[]{:S(2)}, u32[]{:S(2)}) async-start(bf16[4,128,256]{1,2,0:T(8,128)(2,1)} %copy.39), calls=%async_computation | async-start | bytes 524288 | tf_op jit(solution)/shard_map/all_to_all | solution.py:114
  205.8 21.4 %copy-start.7 = (f32[2048]{0:T(1024)S(1)}, f32[2048]{0:T(1024)}, u32[]{:S(2)}) copy-start(f32[2048]{0:T(1024)} %param.27) | copy-start | bytes 24580
  205.8 43.8 %all-to-all-start.2 = ((bf16[32,8,2048]{2,0,1:T(8,128)(2,1)}), bf16[32,8,2048]{2,0,1:T(8,128)(2,1)S(1)}, u32[]{:S(2)}, u32[]{:S(2)}) async-start(bf16[32,8,2048]{2,0,1:T(8,128)(2,1)} %copy.46), calls=%async_computation.3 | async-start | bytes 2097152 | tf_op jit(solution)/shard_map/all_to_all | solution.py:172
  250.2 3.3 %copy-start.8 = (f32[2048]{0:T(1024)S(1)}, f32[2048]{0:T(1024)}, u32[]{:S(2)}) copy-start(f32[2048]{0:T(1024)} %param.35) | copy-start | bytes 24580
Sparse Core Ops, SparseCore 0:
  78.5 33.4 all-gather.5
  114.6 39.4 all-gather.3
  156.6 46.3 reduce-scatter.1
